TPU v7x, 32 devices: a whole 2x2x4 slice. The times are simulated.
32 devices in a mesh: ep: 4 (over y, x), tp: 8 (over z, core).
Axes of the slice: x: 2, y: 2, z: 4, core: 2. Of those that a mesh axis runs over, the one named last changes fastest.
Arguments:
- tokens: bfloat16 [2048, 2048], P('ep', 'tp'), may hold values from -6 to 6
- norm_gain: float32 [2048], replicated, may hold values from 0.1 to 1.9
- norm_shift: float32 [2048], replicated, may hold values from -3 to 3
- expert_ids: int32 [2048, 6], P('ep'), may hold values from 0 to 31, all different within a row; in each aligned block of 64 rows (0 to 63, 64 to 127, ...) at most 24 rows name the same one
- affinity: float32 [2048, 6], P('ep'), may hold values from 0.05 to 1
- expert_gate: bfloat16 [32, 2048, 512], P(('ep', 'tp')), may hold values from -0.125 to 0.125
- expert_up: bfloat16 [32, 2048, 512], P(('ep', 'tp')), may hold values from -0.125 to 0.125
- expert_down: bfloat16 [32, 512, 2048], P(('ep', 'tp')), may hold values from -0.25 to 0.25
- shared_gate: bfloat16 [512, 2048], P('tp'), may hold values from -0.125 to 0.125
- shared_up: bfloat16 [512, 2048], P('tp'), may hold values from -0.125 to 0.125
- shared_down: bfloat16 [512, 2048], replicated, may hold values from -0.25 to 0.25
Outputs:
- mixed: bfloat16 [2048, 2048], P(('ep', 'tp'))
Inputs may be any that keep to these rules, and one draw needn't show every extreme that they name: `expert_ids`: each row names 6 different experts; in each aligned block of 64 rows (the rows of one device of tp) no expert is named more than 24 times, and in some blocks an expert is named exactly 24 times.
All inputs are finite; a program needn't handle non-finite values.
Results may differ from a plain program's by a relative error of at most 0.0069.
Values may be sent and summed in bfloat16 or wider, within the bound.
A program may use at most 64 MiB of HBM per device.

v0:
```python
import jax
import jax.numpy as jnp
from jax import lax
from jax.sharding import PartitionSpec as P

ROUTED_SCALE = 2.5
EPSILON = 1e-05


def pair_ranks(flat_ids, expert_count):
    onehot = flat_ids[..., None] == jnp.arange(expert_count, dtype=jnp.int32)
    running = jnp.cumsum(onehot.astype(jnp.int32), axis=-2)
    return jnp.sum(jnp.where(onehot, running, 0), axis=-1) - 1


def expert_rows(tok_rows, w_gate, w_up, w_down):
    gate_act = jnp.dot(tok_rows, w_gate, preferred_element_type=jnp.float32)
    up_act = jnp.dot(tok_rows, w_up, preferred_element_type=jnp.float32)
    hidden = (jax.nn.silu(gate_act) * up_act).astype(jnp.bfloat16)
    return jnp.dot(hidden, w_down, preferred_element_type=jnp.float32).astype(jnp.bfloat16)


def weighted_sum(source_rows, slot_index, pair_weight, top_count):
    total = jnp.zeros((slot_index.shape[0], source_rows.shape[1]), jnp.float32)
    for column in range(top_count):
        picked = jnp.take(source_rows, slot_index[:, column], axis=0, mode="fill", fill_value=0)
        total = total + pair_weight[:, column : column + 1] * picked.astype(jnp.float32)
    return total


def on_device(
    tokens,
    norm_gain,
    norm_shift,
    expert_ids,
    affinity,
    expert_gate,
    expert_up,
    expert_down,
    shared_gate,
    shared_up,
    shared_down,
):
    ep_count = lax.axis_size("ep")
    tp_count = lax.axis_size("tp")
    tp_index = lax.axis_index("tp")
    whole = lax.all_gather(tokens, "tp", axis=1, tiled=True)
    tok_count = whole.shape[0]
    width = whole.shape[1]
    top_count = expert_ids.shape[1]
    block_rows = tok_count // tp_count
    expert_count = ep_count * tp_count
    slot_cap = max(1, 2 * block_rows * top_count // expert_count)
    slot_total = expert_count * slot_cap
    values = whole.astype(jnp.float32)
    center = values - jnp.mean(values, axis=1, keepdims=True)
    spread = jnp.mean(center * center, axis=1, keepdims=True)
    normed = (center * lax.rsqrt(spread + EPSILON) * norm_gain + norm_shift).astype(jnp.bfloat16)
    weights = affinity / jnp.sum(affinity, axis=1, keepdims=True) * ROUTED_SCALE
    contract = (((1,), (1,)), ((), ()))
    shared_g = lax.dot_general(shared_gate, normed, contract, preferred_element_type=jnp.float32)
    shared_u = lax.dot_general(shared_up, normed, contract, preferred_element_type=jnp.float32)
    shared_hidden = (jax.nn.silu(shared_g) * shared_u).astype(jnp.bfloat16)
    own_hidden = lax.all_to_all(shared_hidden, "tp", split_axis=1, concat_axis=0, tiled=True)
    shared_out = lax.dot_general(
        own_hidden, shared_down, (((0,), (0,)), ((), ())), preferred_element_type=jnp.float32
    )
    block_ids = expert_ids.reshape(tp_count, block_rows * top_count)
    ranks = pair_ranks(block_ids, expert_count)
    group_index = block_ids // tp_count
    mine = block_ids % tp_count == tp_index
    block_index = jnp.arange(tp_count, dtype=jnp.int32)[:, None]
    dest = jnp.where(mine, (group_index * tp_count + block_index) * slot_cap + ranks, slot_total)
    token_index = (
        block_index * block_rows
        + jnp.arange(block_rows * top_count, dtype=jnp.int32)[None, :] // top_count
    )
    source_row = (
        jnp.full((slot_total + 1,), tok_count, jnp.int32)
        .at[dest.reshape(-1)]
        .set(token_index.reshape(-1))[:slot_total]
    )
    outgoing = jnp.take(normed, source_row, axis=0, mode="fill", fill_value=0).reshape(
        ep_count, tp_count, slot_cap, width
    )
    incoming = lax.all_to_all(outgoing, "ep", split_axis=0, concat_axis=0, tiled=True)
    result = expert_rows(incoming.reshape(-1, width), expert_gate[0], expert_up[0], expert_down[0])
    returned = lax.all_to_all(
        result.reshape(incoming.shape), "ep", split_axis=0, concat_axis=0, tiled=True
    )
    pair_slot = dest.reshape(tok_count, top_count)
    back_rows = returned.reshape(slot_total, width)
    routed = lax.psum_scatter(
        weighted_sum(back_rows, pair_slot, weights, top_count),
        "tp",
        scatter_dimension=0,
        tiled=True,
    )
    return (routed + shared_out).astype(jnp.bfloat16)


def solution(mesh):
    placed = (
        P("ep", "tp"),
        P(),
        P(),
        P("ep", None),
        P("ep", None),
        P(("ep", "tp"), None, None),
        P(("ep", "tp"), None, None),
        P(("ep", "tp"), None, None),
        P("tp", None),
        P("tp", None),
        P(),
    )
    return jax.shard_map(
        on_device, mesh=mesh, in_specs=placed, out_specs=P(("ep", "tp"), None), check_vma=False
    )
```

profile of v0, /device:TPU:0, one launch (start us, length us, event | category | flops | bytes accessed | tf_op | source)
XLA Modules:
  0.0 271.8 jit_solution(16597467197731617035)
XLA Ops:
  6.5 0.0 copy-start
  6.5 0.0 all-gather.2.cloned.1.call-start
  6.5 0.7 all-gather.2.cloned.1.call-update
  7.3 0.9 copy.34
  8.1 0.2 eq.48
  8.3 0.2 reshape.242
  8.5 0.2 eq.52
  8.7 0.1 broadcast_add_fusion
  8.8 6.9 %reduce-window.6 = s32[8,32,3,128]{3,1,2,0:T(8,128)S(1)} reduce-window(s32[8,32,3,128]{3,1,2,0:T(8,128)S(1)} %fusion.20, s32[]{:T(128)} %constant.82.clone.1), window={size=1x1x1x128 pad=0_0x0_0x0_0x127_0}, to_apply=%region_1.0 | reduce-window | flops 12484608 | bytes 786436 | tf_op jit(solution)/shard_map/reduce-window
  15.8 0.2 slice.78
  15.9 0.2 copy.40
  16.1 0.1 fusion.29
  16.3 0.2 fusion.19
  16.5 0.1 compare_select_fusion
  16.6 11.8 %scatter_custom_fusion = s32[769]{0:T(1024)S(1)} fusion(s32[3072]{0:T(1024)S(1)} %bitcast.82, s32[3072]{0:T(1024)S(1)} %reshape.307, s32[]{:T(128)} %constant.81.clone.1), kind=kCustom, calls=%fused_computation.94 | custom fusion | bytes 3080 | tf_op jit(solution)/shard_map/scatter | solution.py:81
  28.4 0.1 slice.51
  28.5 13.8 %all-gather.2.cloned.1.call-done = bf16[512,2048]{1,0:T(8,128)(2,1)} async-done(((bf16[512,256]{1,0:T(8,128)(2,1)}), bf16[512,2048]{1,0:T(8,128)(2,1)}) %all-gather.2.cloned.1.call-update) | async-done | bytes 2097168 | tf_op jit(solution)/shard_map/all_gather | solution.py:47
  42.3 0.0 copy-start.2
  42.3 0.0 copy-start.6
  42.3 2.1 convert_reduce_fusion
  44.4 0.1 copy-done.2
  44.5 0.7 fusion.2
  45.2 0.0 copy-done.5
  45.2 0.0 copy-done.6
  45.2 2.2 fusion.5
  47.4 9.0 %gather_fusion = bf16[768,2048]{1,0:T(8,128)(2,1)} fusion(bf16[512,2048]{1,0:T(8,128)(2,1)} %fusion.5, s32[1024]{0:T(1024)S(1)} %pad_clamp_fusion.6), kind=kCustom, calls=%fused_computation.6 | custom fusion | bytes 6294528 | tf_op jit(solution)/shard_map/jit(_take)/gather | solution.py:83
  56.4 3.9 %broadcast_select_fusion = bf16[4,8,24,2048]{3,2,1,0:T(8,128)(2,1)} fusion(bf16[4,8,24,2048]{3,2,1,0:T(8,128)(2,1)} %bitcast.77, pred[4,8,24]{2,1,0:T(8,128)(4,1)S(1)} %compare_and_fusion), kind=kLoop, calls=%fused_computation.18 | loop fusion | flops 1572864 | bytes 6292224 | tf_op jit(solution)/shard_map/jit(_take)/select_n | solution.py:83
  60.3 0.0 copy-start.4
  60.3 4.9 %all-to-all-start = ((bf16[4,8,24,2048]{3,2,1,0:T(8,128)(2,1)}), bf16[4,8,24,2048]{3,2,1,0:T(8,128)(2,1)}, u32[]{:S(2)}, u32[]{:S(2)}) async-start(bf16[4,8,24,2048]{3,2,1,0:T(8,128)(2,1)} %broadcast_select_fusion), calls=%async_computation | async-start | bytes 6291456 | tf_op jit(solution)/shard_map/all_to_all | solution.py:86
  65.2 0.1 add.204
  65.3 0.2 sub.37
  65.5 0.0 copy-done.4
  65.5 0.3 fusion.26
  65.8 0.8 slice_reduce_fusion.5
  66.7 35.2 %all-to-all-done = bf16[4,8,24,2048]{3,2,1,0:T(8,128)(2,1)} async-done(((bf16[4,8,24,2048]{3,2,1,0:T(8,128)(2,1)}), bf16[4,8,24,2048]{3,2,1,0:T(8,128)(2,1)}, u32[]{:S(2)}, u32[]{:S(2)}) %all-to-all-start) | async-done | bytes 3145760 | tf_op jit(solution)/shard_map/all_to_all | solution.py:86
  101.9 5.6 %fusion.10 = f32[768,512]{1,0:T(8,128)} fusion(bf16[768,2048]{1,0:T(8,128)(2,1)} %bitcast.5, bf16[1,2048,512]{2,1,0:T(8,128)(2,1)} %param.18), kind=kOutput, calls=%fused_computation.24 | convolution fusion | flops 1610612736 | bytes 6815744 | tf_op jit(solution)/shard_map/dot_general | solution.py:17
  107.4 0.0 copy-done
  107.4 8.2 %convolution_convert_fusion = bf16[768,2048]{1,0:T(8,128)(2,1)} fusion(bf16[1,512,2048]{2,1,0:T(8,128)(2,1)S(1)} %copy-done, f32[768,512]{1,0:T(8,128)} %fusion.10, bf16[768,2048]{1,0:T(8,128)(2,1)} %bitcast.5, bf16[1,2048,512]{2,1,0:T(8,128)(2,1)} %param.19), kind=kOutput, calls=%fused_computation.17 | convolution fusion | flops 3225157632 | bytes 12058624 | tf_op jit(solution)/shard_map/dot_general | solution.py:20
  115.6 4.6 %all-to-all-start.1 = ((bf16[4,8,24,2048]{3,2,1,0:T(8,128)(2,1)}), bf16[4,8,24,2048]{3,2,1,0:T(8,128)(2,1)}, u32[]{:S(2)}, u32[]{:S(2)}) async-start(bf16[4,8,24,2048]{3,2,1,0:T(8,128)(2,1)} %bitcast.78), calls=%async_computation.1 | async-start | bytes 6291456 | tf_op jit(solution)/shard_map/all_to_all | solution.py:88
  120.3 0.0 reduce-scatter.2.cloned.1.call-start
  120.5 35.7 %all-to-all-done.1 = bf16[4,8,24,2048]{3,2,1,0:T(8,128)(2,1)} async-done(((bf16[4,8,24,2048]{3,2,1,0:T(8,128)(2,1)}), bf16[4,8,24,2048]{3,2,1,0:T(8,128)(2,1)}, u32[]{:S(2)}, u32[]{:S(2)}) %all-to-all-start.1) | async-done | bytes 3145760 | tf_op jit(solution)/shard_map/all_to_all | solution.py:88
  156.2 7.8 %gather_fusion.6 = bf16[512,2048]{1,0:T(8,128)(2,1)} fusion(bf16[768,2048]{1,0:T(8,128)(2,1)} %bitcast.10, s32[1024]{0:T(1024)S(1)} %pad_clamp_fusion), kind=kCustom, calls=%fused_computation.5.clone | custom fusion | bytes 4196352 | tf_op jit(solution)/shard_map/jit(_take)/gather | solution.py:26
  164.0 7.5 %gather_fusion.5 = bf16[512,2048]{1,0:T(8,128)(2,1)} fusion(bf16[768,2048]{1,0:T(8,128)(2,1)} %bitcast.10, s32[1024]{0:T(1024)S(1)} %pad_clamp_fusion.1), kind=kCustom, calls=%fused_computation.4.clone | custom fusion | bytes 4196352 | tf_op jit(solution)/shard_map/jit(_take)/gather | solution.py:26
  171.6 7.5 %gather_fusion.4 = bf16[512,2048]{1,0:T(8,128)(2,1)} fusion(bf16[768,2048]{1,0:T(8,128)(2,1)} %bitcast.10, s32[1024]{0:T(1024)S(1)} %pad_clamp_fusion.2), kind=kCustom, calls=%fused_computation.3.clone | custom fusion | bytes 4196352 | tf_op jit(solution)/shard_map/jit(_take)/gather | solution.py:26
  179.1 7.5 %gather_fusion.3 = bf16[512,2048]{1,0:T(8,128)(2,1)} fusion(bf16[768,2048]{1,0:T(8,128)(2,1)} %bitcast.10, s32[1024]{0:T(1024)S(1)} %pad_clamp_fusion.3), kind=kCustom, calls=%fused_computation.2.clone | custom fusion | bytes 4196352 | tf_op jit(solution)/shard_map/jit(_take)/gather | solution.py:26
  186.6 7.5 %gather_fusion.2 = bf16[512,2048]{1,0:T(8,128)(2,1)} fusion(bf16[768,2048]{1,0:T(8,128)(2,1)} %bitcast.10, s32[1024]{0:T(1024)S(1)} %pad_clamp_fusion.4), kind=kCustom, calls=%fused_computation.1.clone | custom fusion | bytes 4196352 | tf_op jit(solution)/shard_map/jit(_take)/gather | solution.py:26
  194.1 7.8 %gather_fusion.1 = bf16[512,2048]{1,0:T(8,128)(2,1)} fusion(bf16[768,2048]{1,0:T(8,128)(2,1)} %bitcast.10, s32[1024]{0:T(1024)S(1)} %pad_clamp_fusion.5), kind=kCustom, calls=%fused_computation.clone | custom fusion | bytes 4196352 | tf_op jit(solution)/shard_map/jit(_take)/gather | solution.py:26
  202.0 9.0 %multiply_add_fusion = f32[512,2048]{1,0:T(8,128)} fusion(bf16[512,2048]{1,0:T(8,128)(2,1)} %gather_fusion.6, bf16[512,2048]{1,0:T(8,128)(2,1)} %gather_fusion.5, bf16[512,2048]{1,0:T(8,128)(2,1)} %gather_fusion.4, bf16[512,2048]{1,0:T(8,128)(2,1)} %gather_fusion.3, bf16[512,2048]{1,0:T(8,128)(2,1)} %gather_fusion.2, bf16[512,2048]{1,0:T(8,128)(2,1)} %gather_fusion.1, ...), kind=kLoop, calls=%fused_computation.16 | loop fusion | flops 24117248 | bytes 16792576 | tf_op jit(solution)/shard_map/add | solution.py:27
  211.0 0.0 reduce-scatter.2.cloned.1.call-update
  211.1 0.9 copy-done.3
  212.0 0.0 copy-start.1
  212.0 0.0 copy-start.7
  212.0 2.5 convolution_bitcast_fusion.1
  214.5 0.0 copy-done.1
  214.5 0.0 copy-done.7
  214.5 0.8 fusion.15
  215.3 0.1 copy.46
  215.4 0.2 reshape.338
  215.6 11.3 %all_to_all.29 = bf16[8,2,2048]{2,1,0:T(2,128)(2,1)S(1)} all-to-all(bf16[8,2,2048]{2,1,0:T(2,128)(2,1)S(1)} %reshape.338), channel_id=1, replica_groups=mesh['ep'=4,'tp'=8] {'tp'}, dimensions={0} | all-to-all | bytes 131072 | tf_op jit(solution)/shard_map/all_to_all | solution.py:64
  226.9 0.1 reshape.339
  227.0 0.1 copy.45
  227.1 0.1 all_to_all.25
  227.3 34.9 %reduce-scatter.2.cloned.1.call-done = f32[64,2048]{1,0:T(8,128)} async-done(((f32[512,2048]{1,0:T(8,128)}), f32[64,2048]{1,0:T(8,128)}) %reduce-scatter.2.cloned.1.call-update) | async-done | bytes 524304 | tf_op jit(solution)/shard_map/reduce_scatter | solution.py:93
  262.1 2.9 %fusion.6 = bf16[64,2048]{1,0:T(8,128)(2,1)} fusion(f32[64,2048]{1,0:T(8,128)} %reduce-scatter.2.cloned.1.call-done, bf16[512,64]{0,1:T(8,128)(2,1)S(1)} %all_to_all.25, bf16[512,2048]{1,0:T(8,128)(2,1)} %param.23), kind=kOutput, calls=%fused_computation.20 | convolution fusion | flops 134479872 | bytes 2949120 | tf_op jit(solution)/shard_map/dot_general | solution.py:65
  (34 shorter events, 0.3 us)
Async XLA Ops:
  6.5 100.9 %copy-start = (bf16[1,512,2048]{2,1,0:T(8,128)(2,1)S(1)}, bf16[1,512,2048]{2,1,0:T(8,128)(2,1)}, u32[]{:S(2)}) copy-start(bf16[1,512,2048]{2,1,0:T(8,128)(2,1)} %param.20) | copy-start | bytes 6291460
  6.5 35.8 %all-gather.2.cloned.1.call-start = ((), (), s32[]{:S(2)}) async-start(), calls=%async_computation.4 | async-start | bytes 2359296 | tf_op jit(solution)/shard_map/all_gather | solution.py:47
  42.3 2.2 copy-start.2
  42.3 2.9 %copy-start.5 = (f32[2048]{0:T(1024)S(1)}, f32[2048]{0:T(1024)}, u32[]{:S(2)}) copy-start(f32[2048]{0:T(1024)} %param.15) | copy-start | bytes 24580
  42.3 2.9 %copy-start.6 = (f32[2048]{0:T(1024)S(1)}, f32[2048]{0:T(1024)}, u32[]{:S(2)}) copy-start(f32[2048]{0:T(1024)} %param.14) | copy-start | bytes 24580
  60.3 5.3 %copy-start.4 = (f32[512,6]{0,1:T(8,128)S(1)}, f32[512,6]{0,1:T(8,128)}, u32[]{:S(2)}) copy-start(f32[512,6]{0,1:T(8,128)} %param.17) | copy-start | bytes 36868
  60.3 41.6 %all-to-all-start = ((bf16[4,8,24,2048]{3,2,1,0:T(8,128)(2,1)}), bf16[4,8,24,2048]{3,2,1,0:T(8,128)(2,1)}, u32[]{:S(2)}, u32[]{:S(2)}) async-start(bf16[4,8,24,2048]{3,2,1,0:T(8,128)(2,1)} %broadcast_select_fusion), calls=%async_computation | async-start | bytes 6291456 | tf_op jit(solution)/shard_map/all_to_all | solution.py:86
  115.6 40.6 %all-to-all-start.1 = ((bf16[4,8,24,2048]{3,2,1,0:T(8,128)(2,1)}), bf16[4,8,24,2048]{3,2,1,0:T(8,128)(2,1)}, u32[]{:S(2)}, u32[]{:S(2)}) async-start(bf16[4,8,24,2048]{3,2,1,0:T(8,128)(2,1)} %bitcast.78), calls=%async_computation.1 | async-start | bytes 6291456 | tf_op jit(solution)/shard_map/all_to_all | solution.py:88
  120.3 141.9 %reduce-scatter.2.cloned.1.call-start = ((), (), s32[]{:S(2)}) async-start(), calls=%async_computation.5 | async-start | bytes 4718592 | tf_op jit(solution)/shard_map/reduce_scatter | solution.py:93
  211.0 0.9 copy-start.3
  212.0 2.5 copy-start.1
  212.0 2.5 copy-start.7
Sparse Core Ops, SparseCore 0:
  8.9 33.3 all-gather.1
  211.2 50.8 reduce-scatter.1
where the time goes:
time: 273 us; the launch traced here: 272 us
  waiting for transfers between devices  120 us (44%)
  local copies, waits for them, and re-layouts  71.2 us (26%)
  other arithmetic  25.8 us (9%)
  matrix products  19.9 us (7%)
  between operations  13.8 us (5%)
  blocking collectives  11.3 us (4%)
  starting transfers between devices  9.63 us (4%)
    gather x6, local copies, waits for them, and re-layouts, weighted_sum(): jnp.take(source_rows, slot_index[:, column], axis=0, mode='fill', fill_va...  45.7 us
    all_to_all x1, waiting for transfers between devices, on_device(): lax.all_to_all(result.reshape(incoming.shape), 'ep', split_axis=0, concat...  35.7 us
    all_to_all x1, waiting for transfers between devices, on_device(): lax.all_to_all(outgoing, 'ep', split_axis=0, concat_axis=0, tiled=True)  35.2 us
    reduce_scatter x1, waiting for transfers between devices, on_device(): lax.psum_scatter(weighted_sum(back_rows, pair_slot, weights, top_count),...  34.9 us
    all_gather x1, waiting for transfers between devices, on_device(): whole = lax.all_gather(tokens, 'tp', axis=1, tiled=True)  13.8 us
    scatter x1, local copies, waits for them, and re-layouts, on_device(): source_row = jnp.full((slot_total + 1,), tok_count, jnp.int32).at[dest.re...  11.8 us
    all_to_all x1, blocking collectives, on_device(): lax.all_to_all(shared_hidden, 'tp', split_axis=1, concat_axis=0, tiled=True)  11.3 us
    add x1, other arithmetic, weighted_sum(): total + pair_weight[:, column:column + 1] * picked.astype(jnp.float32)  9.05 us
  transfers between devices with their start and end apart: 4, of which 4 were waited for; matrix products, arithmetic and copies ran while one was open for 10% of the time, Pallas kernels for 0%

commit v1 on v0

--- a/solution.py
+++ b/solution.py
@@ -41,10 +41,22 @@
     shared_up,
     shared_down,
 ):
+
+    def _press_table(link_axis, unit):
+        dev_count = lax.axis_size(link_axis)
+        leaves = list(map(lambda ii: (ii, (ii + 1) % dev_count), range(dev_count)))
+        now = [None] * dev_count
+        now[dev_count - 1] = unit
+        for dev_j in range(dev_count - 2, -1, -1):
+            now[dev_j] = lax.ppermute(now[dev_j + 1], axis_name=link_axis, perm=leaves)
+        inter = jnp.concatenate(now, 1)
+        current_value = (lax.axis_index(link_axis) + 1) * unit.shape[1]
+        return jnp.roll(inter, current_value, axis=1)
+
     ep_count = lax.axis_size("ep")
     tp_count = lax.axis_size("tp")
     tp_index = lax.axis_index("tp")
-    whole = lax.all_gather(tokens, "tp", axis=1, tiled=True)
+    whole = _press_table("tp", unit=tokens)
     tok_count = whole.shape[0]
     width = whole.shape[1]
     top_count = expert_ids.shape[1]

time: 273 us -> 302 us (1.11)
  waiting for transfers between devices: 120 us -> 136 us
  local copies, waits for them, and re-layouts: 71.2 us -> 81 us
    ppermute x0 -> x7, waiting for transfers between devices: none -> 38.2 us  [_press_table(): now[dev_j] = lax.ppermute(now[dev_j + 1], axis_name=link_axis, perm=leaves)]
    all_gather x1 -> x0, waiting for transfers between devices: 13.8 us -> none  [on_device(): whole = lax.all_gather(tokens, 'tp', axis=1, tiled=True)]
    unnamed x22 -> x35, local copies, waits for them, and re-layouts: 2.26 us -> 12 us
    all_to_all x1, waiting for transfers between devices: 35.2 us -> 29.4 us  [on_device(): lax.all_to_all(outgoing, 'ep', split_axis=0, concat_axis=0, tiled=True)]
  transfers between devices with their start and end apart: 4 -> 10, of which waited for: 4 -> 8; matrix products, arithmetic and copies ran while one was open for 10% -> 9% of each run, Pallas kernels for 0% -> 0%
where the time goes in v1:
time: 302 us; the launch traced here: 301 us
  waiting for transfers between devices  136 us (45%)
  local copies, waits for them, and re-layouts  81 us (27%)
  other arithmetic  24 us (8%)
  matrix products  21.3 us (7%)
  between operations  14 us (5%)
  blocking collectives  13.2 us (4%)
  starting transfers between devices  10.6 us (4%)
    gather x6, local copies, waits for them, and re-layouts, weighted_sum(): jnp.take(source_rows, slot_index[:, column], axis=0, mode='fill', fill_va...  45.7 us
    ppermute x7, waiting for transfers between devices, _press_table(): now[dev_j] = lax.ppermute(now[dev_j + 1], axis_name=link_axis, perm=leaves)  38.2 us
    all_to_all x1, waiting for transfers between devices, on_device(): lax.all_to_all(result.reshape(incoming.shape), 'ep', split_axis=0, concat...  35.4 us
    reduce_scatter x1, waiting for transfers between devices, on_device(): lax.psum_scatter(weighted_sum(back_rows, pair_slot, weights, top_count),...  33.4 us
    all_to_all x1, waiting for transfers between devices, on_device(): lax.all_to_all(outgoing, 'ep', split_axis=0, concat_axis=0, tiled=True)  29.4 us
    all_to_all x1, blocking collectives, on_device(): lax.all_to_all(shared_hidden, 'tp', split_axis=1, concat_axis=0, tiled=True)  13.2 us
    unnamed x35, local copies, waits for them, and re-layouts  12 us
    scatter x1, local copies, waits for them, and re-layouts, on_device(): source_row = jnp.full((slot_total + 1,), tok_count, jnp.int32).at[dest.re...  11.8 us
  transfers between devices with their start and end apart: 10, of which 8 were waited for; matrix products, arithmetic and copies ran while one was open for 9% of the time, Pallas kernels for 0%

profile of v1, /device:TPU:0, one launch (start us, length us, event | category | flops | bytes accessed | tf_op | source)
XLA Modules:
  0.0 300.7 jit_solution(13491638563608755057)
XLA Ops:
  6.5 0.5 collective-permute-start
  7.0 8.4 %collective-permute-done = bf16[512,256]{1,0:T(8,128)(2,1)} collective-permute-done((bf16[512,256]{1,0:T(8,128)(2,1)}, bf16[512,256]{1,0:T(8,128)(2,1)}, u32[]{:S(2)}, u32[]{:S(2)}) %collective-permute-start) | collective-permute-done | bytes 262176 | tf_op jit(solution)/shard_map/ppermute | solution.py:51
  15.4 0.9 copy.34
  16.3 0.2 eq.51
  16.5 0.2 eq.55
  16.7 6.9 %reduce-window.6 = s32[8,32,3,128]{3,1,2,0:T(8,128)S(1)} reduce-window(s32[8,32,3,128]{3,1,2,0:T(8,128)S(1)} %fusion.20, s32[]{:T(128)} %constant.102.clone.1), window={size=1x1x1x128 pad=0_0x0_0x0_0x127_0}, to_apply=%region_1.2 | reduce-window | flops 12484608 | bytes 786436 | tf_op jit(solution)/shard_map/reduce-window
  23.6 0.2 slice.78
  23.8 0.2 copy.40
  24.0 0.4 collective-permute-start.2
  24.4 0.1 fusion.29
  24.5 0.2 fusion.19
  24.7 7.1 %collective-permute-done.2 = bf16[512,256]{1,0:T(8,128)(2,1)S(1)} collective-permute-done((bf16[512,256]{1,0:T(8,128)(2,1)}, bf16[512,256]{1,0:T(8,128)(2,1)S(1)}, u32[]{:S(2)}, u32[]{:S(2)}) %collective-permute-start.2) | collective-permute-done | bytes 262176 | tf_op jit(solution)/shard_map/ppermute | solution.py:51
  31.9 0.2 reshape.242
  32.1 7.3 %collective-permute-done.3 = bf16[512,256]{1,0:T(8,128)(2,1)S(1)} collective-permute-done((bf16[512,256]{1,0:T(8,128)(2,1)S(1)}, bf16[512,256]{1,0:T(8,128)(2,1)S(1)}, u32[]{:S(2)}, u32[]{:S(2)}) %collective-permute-start.3) | collective-permute-done | bytes 262176 | tf_op jit(solution)/shard_map/ppermute | solution.py:51
  39.5 0.1 compare_select_fusion
  39.6 7.6 %collective-permute-done.4 = bf16[512,256]{1,0:T(8,128)(2,1)} collective-permute-done((bf16[512,256]{1,0:T(8,128)(2,1)S(1)}, bf16[512,256]{1,0:T(8,128)(2,1)}, u32[]{:S(2)}, u32[]{:S(2)}) %collective-permute-start.4) | collective-permute-done | bytes 262176 | tf_op jit(solution)/shard_map/ppermute | solution.py:51
  47.2 0.1 broadcast_add_fusion
  47.2 11.8 %scatter_custom_fusion = s32[769]{0:T(1024)S(1)} fusion(s32[3072]{0:T(1024)S(1)} %bitcast.82, s32[3072]{0:T(1024)S(1)} %reshape.307, s32[]{:T(128)} %constant.101.clone.1), kind=kCustom, calls=%fused_computation.110 | custom fusion | bytes 3080 | tf_op jit(solution)/shard_map/scatter | solution.py:93
  59.0 0.1 collective-permute-start.6
  59.1 0.1 slice.51
  59.2 7.8 %collective-permute-done.6 = bf16[512,256]{1,0:T(8,128)(2,1)} collective-permute-done((bf16[512,256]{1,0:T(8,128)(2,1)}, bf16[512,256]{1,0:T(8,128)(2,1)}, u32[]{:S(2)}, u32[]{:S(2)}) %collective-permute-start.6) | collective-permute-done | bytes 262176 | tf_op jit(solution)/shard_map/ppermute | solution.py:51
  67.0 1.0 constant_dynamic-update-slice_fusion.15
  68.0 1.0 constant_dynamic-update-slice_fusion.14
  69.0 1.0 constant_dynamic-update-slice_fusion.13
  70.0 1.0 constant_dynamic-update-slice_fusion.10
  71.0 1.0 constant_dynamic-update-slice_fusion.9
  72.0 1.0 constant_dynamic-update-slice_fusion.7
  73.0 1.0 constant_dynamic-update-slice_fusion.6
  74.0 1.0 constant_dynamic-update-slice_fusion.5
  75.1 1.0 constant_dynamic-update-slice_fusion.2
  76.1 1.0 constant_dynamic-update-slice_fusion.1
  77.1 0.4 convert_reduce_fusion
  77.5 0.7 fusion.2
  78.2 2.2 fusion.5
  80.4 9.0 %gather_fusion = bf16[768,2048]{1,0:T(8,128)(2,1)} fusion(bf16[512,2048]{1,0:T(8,128)(2,1)} %fusion.5, s32[1024]{0:T(1024)S(1)} %pad_clamp_fusion.6), kind=kCustom, calls=%fused_computation.6 | custom fusion | bytes 6294528 | tf_op jit(solution)/shard_map/jit(_take)/gather | solution.py:95
  89.3 3.9 %broadcast_select_fusion = bf16[4,8,24,2048]{3,2,1,0:T(8,128)(2,1)} fusion(bf16[4,8,24,2048]{3,2,1,0:T(8,128)(2,1)} %bitcast.77, pred[4,8,24]{2,1,0:T(8,128)(4,1)S(1)} %compare_and_fusion), kind=kLoop, calls=%fused_computation.18 | loop fusion | flops 1572864 | bytes 6292224 | tf_op jit(solution)/shard_map/jit(_take)/select_n | solution.py:95
  93.2 4.8 %all-to-all-start = ((bf16[4,8,24,2048]{3,2,1,0:T(8,128)(2,1)}), bf16[4,8,24,2048]{3,2,1,0:T(8,128)(2,1)}, u32[]{:S(2)}, u32[]{:S(2)}) async-start(bf16[4,8,24,2048]{3,2,1,0:T(8,128)(2,1)} %broadcast_select_fusion), calls=%async_computation | async-start | bytes 6291456 | tf_op jit(solution)/shard_map/all_to_all | solution.py:98
  98.0 0.1 add.220
  98.1 0.2 sub.42
  98.3 0.3 fusion.26
  98.6 0.8 slice_reduce_fusion.5
  99.5 29.4 %all-to-all-done = bf16[4,8,24,2048]{3,2,1,0:T(8,128)(2,1)} async-done(((bf16[4,8,24,2048]{3,2,1,0:T(8,128)(2,1)}), bf16[4,8,24,2048]{3,2,1,0:T(8,128)(2,1)}, u32[]{:S(2)}, u32[]{:S(2)}) %all-to-all-start) | async-done | bytes 3145760 | tf_op jit(solution)/shard_map/all_to_all | solution.py:98
  128.9 5.6 %fusion.10 = f32[768,512]{1,0:T(8,128)} fusion(bf16[768,2048]{1,0:T(8,128)(2,1)} %bitcast.5, bf16[1,2048,512]{2,1,0:T(8,128)(2,1)} %param.18), kind=kOutput, calls=%fused_computation.24 | convolution fusion | flops 1610612736 | bytes 6815744 | tf_op jit(solution)/shard_map/dot_general | solution.py:17
  134.5 8.2 %convolution_convert_fusion = bf16[768,2048]{1,0:T(8,128)(2,1)} fusion(bf16[1,512,2048]{2,1,0:T(8,128)(2,1)S(1)} %copy-done, f32[768,512]{1,0:T(8,128)} %fusion.10, bf16[768,2048]{1,0:T(8,128)(2,1)} %bitcast.5, bf16[1,2048,512]{2,1,0:T(8,128)(2,1)} %param.19), kind=kOutput, calls=%fused_computation.17 | convolution fusion | flops 3225157632 | bytes 12058624 | tf_op jit(solution)/shard_map/dot_general | solution.py:20
  142.6 4.8 %all-to-all-start.1 = ((bf16[4,8,24,2048]{3,2,1,0:T(8,128)(2,1)}), bf16[4,8,24,2048]{3,2,1,0:T(8,128)(2,1)}, u32[]{:S(2)}, u32[]{:S(2)}) async-start(bf16[4,8,24,2048]{3,2,1,0:T(8,128)(2,1)} %bitcast.78), calls=%async_computation.1 | async-start | bytes 6291456 | tf_op jit(solution)/shard_map/all_to_all | solution.py:100
  147.7 35.4 %all-to-all-done.1 = bf16[4,8,24,2048]{3,2,1,0:T(8,128)(2,1)} async-done(((bf16[4,8,24,2048]{3,2,1,0:T(8,128)(2,1)}), bf16[4,8,24,2048]{3,2,1,0:T(8,128)(2,1)}, u32[]{:S(2)}, u32[]{:S(2)}) %all-to-all-start.1) | async-done | bytes 3145760 | tf_op jit(solution)/shard_map/all_to_all | solution.py:100
  183.1 7.8 %gather_fusion.6 = bf16[512,2048]{1,0:T(8,128)(2,1)} fusion(bf16[768,2048]{1,0:T(8,128)(2,1)} %bitcast.10, s32[1024]{0:T(1024)S(1)} %get-tuple-element.22), kind=kCustom, calls=%fused_computation.5.clone | custom fusion | bytes 4196352 | tf_op jit(solution)/shard_map/jit(_take)/gather | solution.py:26
  190.9 7.5 %gather_fusion.5 = bf16[512,2048]{1,0:T(8,128)(2,1)} fusion(bf16[768,2048]{1,0:T(8,128)(2,1)} %bitcast.10, s32[1024]{0:T(1024)S(1)} %get-tuple-element.23), kind=kCustom, calls=%fused_computation.4.clone | custom fusion | bytes 4196352 | tf_op jit(solution)/shard_map/jit(_take)/gather | solution.py:26
  198.4 7.5 %gather_fusion.4 = bf16[512,2048]{1,0:T(8,128)(2,1)} fusion(bf16[768,2048]{1,0:T(8,128)(2,1)} %bitcast.10, s32[1024]{0:T(1024)S(1)} %get-tuple-element.24), kind=kCustom, calls=%fused_computation.3.clone | custom fusion | bytes 4196352 | tf_op jit(solution)/shard_map/jit(_take)/gather | solution.py:26
  206.0 7.5 %gather_fusion.3 = bf16[512,2048]{1,0:T(8,128)(2,1)} fusion(bf16[768,2048]{1,0:T(8,128)(2,1)} %bitcast.10, s32[1024]{0:T(1024)S(1)} %get-tuple-element.25), kind=kCustom, calls=%fused_computation.2.clone | custom fusion | bytes 4196352 | tf_op jit(solution)/shard_map/jit(_take)/gather | solution.py:26
  213.5 7.5 %gather_fusion.2 = bf16[512,2048]{1,0:T(8,128)(2,1)} fusion(bf16[768,2048]{1,0:T(8,128)(2,1)} %bitcast.10, s32[1024]{0:T(1024)S(1)} %get-tuple-element.26), kind=kCustom, calls=%fused_computation.1.clone | custom fusion | bytes 4196352 | tf_op jit(solution)/shard_map/jit(_take)/gather | solution.py:26
  221.0 7.8 %gather_fusion.1 = bf16[512,2048]{1,0:T(8,128)(2,1)} fusion(bf16[768,2048]{1,0:T(8,128)(2,1)} %bitcast.10, s32[1024]{0:T(1024)S(1)} %get-tuple-element.27), kind=kCustom, calls=%fused_computation.clone | custom fusion | bytes 4196352 | tf_op jit(solution)/shard_map/jit(_take)/gather | solution.py:26
  228.9 9.1 %multiply_add_fusion = f32[512,2048]{1,0:T(8,128)} fusion(bf16[512,2048]{1,0:T(8,128)(2,1)} %gather_fusion.6, bf16[512,2048]{1,0:T(8,128)(2,1)} %gather_fusion.5, bf16[512,2048]{1,0:T(8,128)(2,1)} %gather_fusion.4, bf16[512,2048]{1,0:T(8,128)(2,1)} %gather_fusion.3, bf16[512,2048]{1,0:T(8,128)(2,1)} %gather_fusion.2, bf16[512,2048]{1,0:T(8,128)(2,1)} %gather_fusion.1, ...), kind=kLoop, calls=%fused_computation.16 | loop fusion | flops 24117248 | bytes 16792576 | tf_op jit(solution)/shard_map/add | solution.py:27
  237.9 0.9 copy-done.2
  238.9 2.3 convolution_bitcast_fusion.1
  241.2 2.4 fusion.15
  243.6 0.1 copy.46
  243.7 0.2 reshape.338
  243.9 13.2 %all_to_all.29 = bf16[8,2,2048]{2,1,0:T(2,128)(2,1)S(1)} all-to-all(bf16[8,2,2048]{2,1,0:T(2,128)(2,1)S(1)} %reshape.338), channel_id=1, replica_groups=mesh['ep'=4,'tp'=8] {'tp'}, dimensions={0} | all-to-all | bytes 131072 | tf_op jit(solution)/shard_map/all_to_all | solution.py:76
  257.1 0.1 reshape.339
  257.3 0.1 copy.45
  257.4 0.1 all_to_all.25
  257.5 33.4 %reduce-scatter.2.cloned.1.call-done = f32[64,2048]{1,0:T(8,128)} async-done(((f32[512,2048]{1,0:T(8,128)}), f32[64,2048]{1,0:T(8,128)}) %reduce-scatter.2.cloned.1.call-update) | async-done | bytes 524304 | tf_op jit(solution)/shard_map/reduce_scatter | solution.py:105
  290.9 2.9 fusion.6
  (59 shorter events, 0.5 us)
Async XLA Ops:
  6.5 127.9 %copy-start = (bf16[1,512,2048]{2,1,0:T(8,128)(2,1)S(1)}, bf16[1,512,2048]{2,1,0:T(8,128)(2,1)}, u32[]{:S(2)}) copy-start(bf16[1,512,2048]{2,1,0:T(8,128)(2,1)} %param.20) | copy-start | bytes 6291460
  6.5 8.9 %collective-permute-start = (bf16[512,256]{1,0:T(8,128)(2,1)}, bf16[512,256]{1,0:T(8,128)(2,1)}, u32[]{:S(2)}, u32[]{:S(2)}) collective-permute-start(bf16[512,256]{1,0:T(8,128)(2,1)} %param.13), channel_id=1, source_target_pairs={{0,1},{1,2},{2,3},{3,4},{4,5},{5,6},{6,7},{7,0},{8,9},{9,10},{10,1... | collective-permute-start | bytes 786440 | tf_op jit(solution)/shard_map/ppermute | solution.py:51
  15.4 8.6 %collective-permute-start.1 = (bf16[512,256]{1,0:T(8,128)(2,1)}, bf16[512,256]{1,0:T(8,128)(2,1)}, u32[]{:S(2)}, u32[]{:S(2)}) collective-permute-start(bf16[512,256]{1,0:T(8,128)(2,1)} %collective-permute-done), channel_id=1, source_target_pairs={{0,1},{1,2},{2,3},{3,4},{4,5},{5,6},{6,7},{7,0},{8,9},{9,10},{10,1... | collective-permute-start | bytes 786440 | tf_op jit(solution)/shard_map/ppermute | solution.py:51
  23.6 48.4 %copy-start.1 = (bf16[512,256]{1,0:T(8,128)(2,1)S(1)}, bf16[512,256]{1,0:T(8,128)(2,1)}, u32[]{:S(2)}) copy-start(bf16[512,256]{1,0:T(8,128)(2,1)} %param.13) | copy-start | bytes 786436
  24.0 7.9 %collective-permute-start.2 = (bf16[512,256]{1,0:T(8,128)(2,1)}, bf16[512,256]{1,0:T(8,128)(2,1)S(1)}, u32[]{:S(2)}, u32[]{:S(2)}) collective-permute-start(bf16[512,256]{1,0:T(8,128)(2,1)} %collective-permute-done.1), channel_id=1, source_target_pairs={{0,1},{1,2},{2,3},{3,4},{4,5},{5,6},{6,7},{7,0},{8,9},{9,10},{10,1... | collective-permute-start | bytes 786440 | tf_op jit(solution)/shard_map/ppermute | solution.py:51
  31.9 7.6 %collective-permute-start.3 = (bf16[512,256]{1,0:T(8,128)(2,1)S(1)}, bf16[512,256]{1,0:T(8,128)(2,1)S(1)}, u32[]{:S(2)}, u32[]{:S(2)}) collective-permute-start(bf16[512,256]{1,0:T(8,128)(2,1)S(1)} %collective-permute-done.2), channel_id=1, source_target_pairs={{0,1},{1,2},{2,3},{3,4},{4,5},{5,6},{6,7},{7,0},{8,9},{9,10},{10,1... | collective-permute-start | bytes 786440 | tf_op jit(solution)/shard_map/ppermute | solution.py:51
  39.5 7.7 %collective-permute-start.4 = (bf16[512,256]{1,0:T(8,128)(2,1)S(1)}, bf16[512,256]{1,0:T(8,128)(2,1)}, u32[]{:S(2)}, u32[]{:S(2)}) collective-permute-start(bf16[512,256]{1,0:T(8,128)(2,1)S(1)} %collective-permute-done.3), channel_id=1, source_target_pairs={{0,1},{1,2},{2,3},{3,4},{4,5},{5,6},{6,7},{7,0},{8,9},{9,10},{10,1... | collective-permute-start | bytes 786440 | tf_op jit(solution)/shard_map/ppermute | solution.py:51
  47.2 11.9 %collective-permute-start.5 = (bf16[512,256]{1,0:T(8,128)(2,1)}, bf16[512,256]{1,0:T(8,128)(2,1)}, u32[]{:S(2)}, u32[]{:S(2)}) collective-permute-start(bf16[512,256]{1,0:T(8,128)(2,1)} %collective-permute-done.4), channel_id=1, source_target_pairs={{0,1},{1,2},{2,3},{3,4},{4,5},{5,6},{6,7},{7,0},{8,9},{9,10},{10,1... | collective-permute-start | bytes 786440 | tf_op jit(solution)/shard_map/ppermute | solution.py:51
  59.0 8.0 %collective-permute-start.6 = (bf16[512,256]{1,0:T(8,128)(2,1)}, bf16[512,256]{1,0:T(8,128)(2,1)}, u32[]{:S(2)}, u32[]{:S(2)}) collective-permute-start(bf16[512,256]{1,0:T(8,128)(2,1)} %collective-permute-done.5), channel_id=1, source_target_pairs={{0,1},{1,2},{2,3},{3,4},{4,5},{5,6},{6,7},{7,0},{8,9},{9,10},{10,1... | collective-permute-start | bytes 786440 | tf_op jit(solution)/shard_map/ppermute | solution.py:51
  75.0 3.1 %copy-start.4 = (f32[2048]{0:T(1024)S(1)}, f32[2048]{0:T(1024)}, u32[]{:S(2)}) copy-start(f32[2048]{0:T(1024)} %param.15) | copy-start | bytes 24580
  75.0 3.1 %copy-start.5 = (f32[2048]{0:T(1024)S(1)}, f32[2048]{0:T(1024)}, u32[]{:S(2)}) copy-start(f32[2048]{0:T(1024)} %param.14) | copy-start | bytes 24580
  93.2 35.7 %all-to-all-start = ((bf16[4,8,24,2048]{3,2,1,0:T(8,128)(2,1)}), bf16[4,8,24,2048]{3,2,1,0:T(8,128)(2,1)}, u32[]{:S(2)}, u32[]{:S(2)}) async-start(bf16[4,8,24,2048]{3,2,1,0:T(8,128)(2,1)} %broadcast_select_fusion), calls=%async_computation | async-start | bytes 6291456 | tf_op jit(solution)/shard_map/all_to_all | solution.py:98
  142.6 4.8 %copy-start.3 = (f32[512,6]{0,1:T(8,128)S(1)}, f32[512,6]{0,1:T(8,128)}, u32[]{:S(2)}) copy-start(f32[512,6]{0,1:T(8,128)} %param.17) | copy-start | bytes 36868
  142.6 40.5 %all-to-all-start.1 = ((bf16[4,8,24,2048]{3,2,1,0:T(8,128)(2,1)}), bf16[4,8,24,2048]{3,2,1,0:T(8,128)(2,1)}, u32[]{:S(2)}, u32[]{:S(2)}) async-start(bf16[4,8,24,2048]{3,2,1,0:T(8,128)(2,1)} %bitcast.78), calls=%async_computation.1 | async-start | bytes 6291456 | tf_op jit(solution)/shard_map/all_to_all | solution.py:100
  147.4 143.5 %reduce-scatter.2.cloned.1.call-start = ((), (), s32[]{:S(2)}) async-start(), calls=%async_computation.4 | async-start | bytes 4718592 | tf_op jit(solution)/shard_map/reduce_scatter | solution.py:105
  237.9 0.9 copy-start.2
  237.9 3.3 %copy-start.6 = (bf16[64,2048]{1,0:T(8,128)(2,1)S(1)}, bf16[64,2048]{1,0:T(8,128)(2,1)}, u32[]{:S(2)}) copy-start(bf16[64,2048]{1,0:T(8,128)(2,1)} %param.22) | copy-start | bytes 786436
Sparse Core Ops, SparseCore 0:
  238.1 52.8 reduce-scatter.1
